TPU v7x, 32 devices: a whole 2x2x4 slice. The times are simulated.
32 devices in a mesh: fs: 8 (over z, y), tp: 4 (over x, core).
Axes of the slice: x: 2, y: 2, z: 4, core: 2. Of those that a mesh axis runs over, the one named last changes fastest.
Arguments:
- tokens: bfloat16 [8192, 2048], P('fs', 'tp'), may hold values from -6 to 6
- norm_gain: float32 [2048], P('fs'), may hold values from 0.1 to 1.9
- up_master: float32 [2048, 4096], P('fs', 'tp'), may hold values from -0.125 to 0.125
- down_master: float32 [4096, 2048], P('fs', 'tp'), may hold values from -0.09375 to 0.09375
Outputs:
- mixed: bfloat16 [8192, 2048], P('fs', 'tp')
- up_ready: bfloat16 [2048, 4096], P(None, 'tp')
- down_ready: bfloat16 [4096, 2048], P('tp')
All inputs are finite; a program needn't handle non-finite values.
Results may differ from a plain program's by a relative error of at most 0.0095.
Values may be sent and summed in bfloat16 or wider, within the bound.
A program may use at most 128 MiB of HBM per device.

v0:
```python
import jax
import jax.numpy as jnp
from jax import lax
from jax.sharding import PartitionSpec as P


def shards(tokens, norm_gain, up_master, down_master):
    up_local = (norm_gain[:, None] * up_master).astype(jnp.bfloat16)
    up_ready = lax.all_gather(up_local, "fs", axis=0, tiled=True)
    down_local = down_master.astype(jnp.bfloat16)
    gathered = lax.all_gather(down_local, "fs", axis=0, tiled=True)
    down_ready = lax.all_to_all(gathered, "tp", split_axis=0, concat_axis=1, tiled=True)
    features = lax.all_gather(tokens, "tp", axis=1, tiled=True)
    values = features.astype(jnp.float32)
    mean_square = jnp.mean(values * values, axis=-1, keepdims=True)
    normed = (values * lax.rsqrt(mean_square + 1e-06)).astype(jnp.bfloat16)
    before = jnp.dot(normed, up_ready, preferred_element_type=jnp.float32)
    hidden = jnp.square(jax.nn.relu(before)).astype(jnp.bfloat16)
    partial_value = jnp.dot(hidden, down_ready, preferred_element_type=jnp.float32)
    mixed = lax.psum_scatter(
        partial_value.astype(jnp.bfloat16), "tp", scatter_dimension=1, tiled=True
    )
    return (mixed, up_ready, down_ready)


def solution(mesh):
    return jax.shard_map(
        shards,
        mesh=mesh,
        in_specs=(P("fs", "tp"), P("fs"), P("fs", "tp"), P("fs", "tp")),
        out_specs=(P("fs", "tp"), P(None, "tp"), P("tp", None)),
        check_vma=False,
    )
```

profile of v0, /device:TPU:0, one launch (start us, length us, event | category | flops | bytes accessed | tf_op | source)
XLA Modules:
  0.0 287.9 jit_solution(17428654618168584598)
XLA Ops:
  7.2 0.0 all-gather.8.cloned.1.call-start
  7.2 2.1 convert_element_type.22
  9.3 0.0 all-gather.8.cloned.1.call-update
  9.3 0.0 all-gather.4.cloned.1.call-start
  9.4 0.7 all-gather.4.cloned.1.call-update
  10.1 0.0 all-gather.6.cloned.1.call-start
  10.1 2.1 multiply_convert_fusion.2
  12.3 0.0 all-gather.6.cloned.1.call-update
  12.3 73.9 %all-gather.8.cloned.1.call-done = bf16[4096,512]{1,0:T(8,128)(2,1)} async-done(((bf16[512,512]{1,0:T(8,128)(2,1)}), bf16[4096,512]{1,0:T(8,128)(2,1)}) %all-gather.8.cloned.1.call-update) | async-done | bytes 4194320 | tf_op jit(solution)/shard_map/all_gather | solution.py:11
  86.2 4.9 %all-to-all-start = ((bf16[4,1024,512]{2,1,0:T(8,128)(2,1)}), bf16[4,1024,512]{2,1,0:T(8,128)(2,1)}, u32[]{:S(2)}, u32[]{:S(2)}) async-start(bf16[4,1024,512]{2,1,0:T(8,128)(2,1)} %bitcast.8), calls=%async_computation | async-start | bytes 8388608 | tf_op jit(solution)/shard_map/all_to_all | solution.py:12
  91.1 0.0 reduce-scatter.2.cloned.1.call-start
  91.2 52.2 %all-gather.4.cloned.1.call-done = bf16[1024,2048]{1,0:T(8,128)(2,1)} async-done(((bf16[1024,512]{1,0:T(8,128)(2,1)}), bf16[1024,2048]{1,0:T(8,128)(2,1)}) %all-gather.4.cloned.1.call-update) | async-done | bytes 4194320 | tf_op jit(solution)/shard_map/all_gather | solution.py:13
  143.4 3.1 %fusion = f32[1024]{0:T(1024)S(1)} fusion(bf16[1024,2048]{1,0:T(8,128)(2,1)} %all-gather.4.cloned.1.call-done), kind=kLoop, calls=%fused_computation.2 | loop fusion | flops 6290432 | bytes 4198400 | tf_op jit(solution)/shard_map/reduce_sum | solution.py:15
  146.5 15.3 %all-to-all-done = bf16[4,1024,512]{2,1,0:T(8,128)(2,1)} async-done(((bf16[4,1024,512]{2,1,0:T(8,128)(2,1)}), bf16[4,1024,512]{2,1,0:T(8,128)(2,1)}, u32[]{:S(2)}, u32[]{:S(2)}) %all-to-all-start) | async-done | bytes 4194336 | tf_op jit(solution)/shard_map/all_to_all | solution.py:12
  161.8 6.2 %copy.8 = bf16[4,1024,512]{1,2,0:T(8,128)(2,1)} copy(bf16[4,1024,512]{2,1,0:T(8,128)(2,1)} %all-to-all-done) | data formatting | bytes 8388608 | tf_op jit(solution)/shard_map/all_to_all | solution.py:12
  168.0 50.9 %all-gather.6.cloned.1.call-done = bf16[2048,1024]{1,0:T(8,128)(2,1)} async-done(((bf16[256,1024]{1,0:T(8,128)(2,1)}), bf16[2048,1024]{1,0:T(8,128)(2,1)}) %all-gather.6.cloned.1.call-update) | async-done | bytes 4194320 | tf_op jit(solution)/shard_map/all_gather | solution.py:9
  218.9 14.7 %convolution_convert_fusion = bf16[1024,2048]{1,0:T(8,128)(2,1)} fusion(bf16[1024,2048]{0,1:T(8,128)(2,1)} %bitcast.6, bf16[2048,1024]{1,0:T(8,128)(2,1)} %all-gather.6.cloned.1.call-done, bf16[1024,2048]{1,0:T(8,128)(2,1)} %all-gather.4.cloned.1.call-done, f32[1024]{0:T(1024)S(1)} %add_rsqrt_fusion), kind=kOutput, calls=%fused_computation.7 | convolution fusion | flops 8601468928 | bytes 16781312 | tf_op jit(solution)/shard_map/dot_general | solution.py:19
  233.6 0.0 reduce-scatter.2.cloned.1.call-update
  233.6 6.5 %copy.9 = bf16[1024,2048]{1,0:T(8,128)(2,1)} copy(bf16[1024,2048]{0,1:T(8,128)(2,1)} %bitcast.7) | data formatting | bytes 8388608
  240.1 36.6 %reduce-scatter.2.cloned.1.call-done = bf16[1024,512]{1,0:T(8,128)(2,1)} async-done(((bf16[1024,2048]{1,0:T(8,128)(2,1)}), bf16[1024,512]{1,0:T(8,128)(2,1)}) %reduce-scatter.2.cloned.1.call-update) | async-done | bytes 1048592 | tf_op jit(solution)/shard_map/reduce_scatter | solution.py:20
  276.7 4.6 %copy.11 = bf16[2048,1024]{1,0:T(8,128)(2,1)} copy(bf16[2048,1024]{1,0:T(8,128)(2,1)} %all-gather.6.cloned.1.call-done) | data formatting | bytes 8388608
  (1 shorter events, 0.0 us)
Async XLA Ops:
  7.2 79.1 %all-gather.8.cloned.1.call-start = ((), (), s32[]{:S(2)}) async-start(), calls=%async_computation.4 | async-start | bytes 4718592 | tf_op jit(solution)/shard_map/all_gather | solution.py:11
  9.3 134.1 %all-gather.4.cloned.1.call-start = ((), (), s32[]{:S(2)}) async-start(), calls=%async_computation.2 | async-start | bytes 5242880 | tf_op jit(solution)/shard_map/all_gather | solution.py:13
  10.1 208.8 %all-gather.6.cloned.1.call-start = ((), (), s32[]{:S(2)}) async-start(), calls=%async_computation.3 | async-start | bytes 4718592 | tf_op jit(solution)/shard_map/all_gather | solution.py:9
  86.2 75.6 %all-to-all-start = ((bf16[4,1024,512]{2,1,0:T(8,128)(2,1)}), bf16[4,1024,512]{2,1,0:T(8,128)(2,1)}, u32[]{:S(2)}, u32[]{:S(2)}) async-start(bf16[4,1024,512]{2,1,0:T(8,128)(2,1)} %bitcast.8), calls=%async_computation | async-start | bytes 8388608 | tf_op jit(solution)/shard_map/all_to_all | solution.py:12
  91.1 185.6 %reduce-scatter.2.cloned.1.call-start = ((), (), s32[]{:S(2)}) async-start(), calls=%async_computation.5 | async-start | bytes 5242880 | tf_op jit(solution)/shard_map/reduce_scatter | solution.py:20
Sparse Core Ops, SparseCore 0:
  10.7 75.5 all-gather.7
  87.8 55.5 all-gather.3
  146.1 72.7 all-gather.5
  233.7 42.9 reduce-scatter.1
where the time goes:
time: 288 us
  waiting for transfers between devices  230 us (80%)
  local copies, waits for them, and re-layouts  17.3 us (6%)
  matrix products  14.7 us (5%)
  between operations  13.8 us (5%)
  other arithmetic  7.31 us (3%)
  starting transfers between devices  5.06 us (2%)
    all_gather x1, waiting for transfers between devices, shards(): gathered = lax.all_gather(down_local, 'fs', axis=0, tiled=True)  73.9 us
    all_gather x1, waiting for transfers between devices, shards(): features = lax.all_gather(tokens, 'tp', axis=1, tiled=True)  52.2 us
    all_gather x1, waiting for transfers between devices, shards(): up_ready = lax.all_gather(up_local, 'fs', axis=0, tiled=True)  50.9 us
    reduce_scatter x1, waiting for transfers between devices, shards(): lax.psum_scatter(partial_value.astype(jnp.bfloat16), 'tp', scatter_dimens...  36.6 us
    all_to_all x1, waiting for transfers between devices, shards(): lax.all_to_all(gathered, 'tp', split_axis=0, concat_axis=1, tiled=True)  15.3 us
    dot_general x1, matrix products, shards(): jnp.dot(hidden, down_ready, preferred_element_type=jnp.float32)  14.7 us
    unnamed x2, local copies, waits for them, and re-layouts  11.1 us
    all_to_all x1, local copies, waits for them, and re-layouts, shards(): lax.all_to_all(gathered, 'tp', split_axis=0, concat_axis=1, tiled=True)  6.21 us
  transfers between devices with their start and end apart: 5, of which 5 were waited for; matrix products, arithmetic and copies ran while one was open for 6% of the time, Pallas kernels for 0%

commit v1 on v0

--- a/solution.py
+++ b/solution.py
@@ -8,7 +8,12 @@
     up_local = (norm_gain[:, None] * up_master).astype(jnp.bfloat16)
     up_ready = lax.all_gather(up_local, "fs", axis=0, tiled=True)
     down_local = down_master.astype(jnp.bfloat16)
-    gathered = lax.all_gather(down_local, "fs", axis=0, tiled=True)
+    ring = [down_local]
+    for hop in range(7):
+        ring.append(lax.ppermute(ring[-1], "fs", [(dev, (dev + 1) % 8) for dev in range(8)]))
+    gathered = jnp.roll(
+        jnp.concatenate(ring[::-1], axis=0), (lax.axis_index("fs") + 1) * ring[0].shape[0], axis=0
+    )
     down_ready = lax.all_to_all(gathered, "tp", split_axis=0, concat_axis=1, tiled=True)
     features = lax.all_gather(tokens, "tp", axis=1, tiled=True)
     values = features.astype(jnp.float32)

time: 288 us -> 262 us (0.910)
  waiting for transfers between devices: 230 us -> 192 us
  local copies, waits for them, and re-layouts: 17.3 us -> 26.5 us
  starting transfers between devices: 5.06 us -> 8.12 us
    ppermute x0 -> x7, waiting for transfers between devices: none -> 112 us  [shards(): lax.ppermute(ring[-1], 'fs', [(dev, (dev + 1) % 8) for dev in range(8)])]
    all_gather x1 -> x0, waiting for transfers between devices: 73.9 us -> none  [shards(): gathered = lax.all_gather(down_local, 'fs', axis=0, tiled=True)]
    all_gather x1, waiting for transfers between devices: 52.2 us -> 0.02 us  [shards(): features = lax.all_gather(tokens, 'tp', axis=1, tiled=True)]
    all_gather x1, waiting for transfers between devices: 50.9 us -> 0.01 us  [shards(): up_ready = lax.all_gather(up_local, 'fs', axis=0, tiled=True)]
    all_to_all x1, waiting for transfers between devices: 15.3 us -> 45 us  [shards(): lax.all_to_all(gathered, 'tp', split_axis=0, concat_axis=1, tiled=True)]
    unnamed x2 -> x18, local copies, waits for them, and re-layouts: 11.1 us -> 18 us
    ppermute x0 -> x7, starting transfers between devices: none -> 3.06 us  [shards(): lax.ppermute(ring[-1], 'fs', [(dev, (dev + 1) % 8) for dev in range(8)])]
  transfers between devices with their start and end apart: 5 -> 11, of which waited for: 5 -> 9; matrix products, arithmetic and copies ran while one was open for 6% -> 11% of each run, Pallas kernels for 0% -> 0%
where the time goes in v1:
time: 262 us
  waiting for transfers between devices  192 us (73%)
  local copies, waits for them, and re-layouts  26.5 us (10%)
  matrix products  14.7 us (6%)
  between operations  13.9 us (5%)
  starting transfers between devices  8.12 us (3%)
  other arithmetic  6.65 us (3%)
    ppermute x7, waiting for transfers between devices, shards(): lax.ppermute(ring[-1], 'fs', [(dev, (dev + 1) % 8) for dev in range(8)])  112 us
    all_to_all x1, waiting for transfers between devices, shards(): lax.all_to_all(gathered, 'tp', split_axis=0, concat_axis=1, tiled=True)  45 us
    reduce_scatter x1, waiting for transfers between devices, shards(): lax.psum_scatter(partial_value.astype(jnp.bfloat16), 'tp', scatter_dimens...  34 us
    unnamed x18, local copies, waits for them, and re-layouts  18 us
    dot_general x1, matrix products, shards(): jnp.dot(hidden, down_ready, preferred_element_type=jnp.float32)  14.7 us
    all_to_all x1, local copies, waits for them, and re-layouts, shards(): lax.all_to_all(gathered, 'tp', split_axis=0, concat_axis=1, tiled=True)  6.19 us
  transfers between devices with their start and end apart: 11, of which 9 were waited for; matrix products, arithmetic and copies ran while one was open for 11% of the time, Pallas kernels for 0%

profile of v1, /device:TPU:0, one launch (start us, length us, event | category | flops | bytes accessed | tf_op | source)
XLA Modules:
  0.0 261.5 jit_solution(13144986197672626581)
XLA Ops:
  7.2 0.0 copy-start
  7.2 0.0 all-gather.3.cloned.1.call-start
  7.2 0.7 all-gather.3.cloned.1.call-update
  7.9 0.0 all-gather.5.cloned.1.call-start
  8.0 1.3 convert_element_type.22
  9.2 3.0 %collective-permute-start = (bf16[512,512]{1,0:T(8,128)(2,1)S(1)}, bf16[512,512]{1,0:T(8,128)(2,1)S(1)}, u32[]{:S(2)}, u32[]{:S(2)}) collective-permute-start(bf16[512,512]{1,0:T(8,128)(2,1)S(1)} %convert_element_type.22), channel_id=1, source_target_pairs={{0,4},{4,8},{8,12},{12,16},{16,20},{20,24},{24,28},{28,0},{1,5},{5... | collective-permute-start | bytes 1572872 | tf_op jit(solution)/shard_map/ppermute | solution.py:13
  12.3 15.0 %collective-permute-done = bf16[512,512]{1,0:T(8,128)(2,1)S(1)} collective-permute-done((bf16[512,512]{1,0:T(8,128)(2,1)S(1)}, bf16[512,512]{1,0:T(8,128)(2,1)S(1)}, u32[]{:S(2)}, u32[]{:S(2)}) %collective-permute-start) | collective-permute-done | bytes 524320 | tf_op jit(solution)/shard_map/ppermute | solution.py:13
  27.3 0.0 collective-permute-start.1
  27.3 15.8 %collective-permute-done.1 = bf16[512,512]{1,0:T(8,128)(2,1)S(1)} collective-permute-done((bf16[512,512]{1,0:T(8,128)(2,1)S(1)}, bf16[512,512]{1,0:T(8,128)(2,1)S(1)}, u32[]{:S(2)}, u32[]{:S(2)}) %collective-permute-start.1) | collective-permute-done | bytes 524320 | tf_op jit(solution)/shard_map/ppermute | solution.py:13
  43.0 0.0 collective-permute-start.2
  43.0 14.9 %collective-permute-done.2 = bf16[512,512]{1,0:T(8,128)(2,1)S(1)} collective-permute-done((bf16[512,512]{1,0:T(8,128)(2,1)S(1)}, bf16[512,512]{1,0:T(8,128)(2,1)S(1)}, u32[]{:S(2)}, u32[]{:S(2)}) %collective-permute-start.2) | collective-permute-done | bytes 524320 | tf_op jit(solution)/shard_map/ppermute | solution.py:13
  58.0 0.0 collective-permute-start.3
  58.0 14.1 %collective-permute-done.3 = bf16[512,512]{1,0:T(8,128)(2,1)S(1)} collective-permute-done((bf16[512,512]{1,0:T(8,128)(2,1)S(1)}, bf16[512,512]{1,0:T(8,128)(2,1)S(1)}, u32[]{:S(2)}, u32[]{:S(2)}) %collective-permute-start.3) | collective-permute-done | bytes 524320 | tf_op jit(solution)/shard_map/ppermute | solution.py:13
  72.0 0.0 collective-permute-start.4
  72.1 2.1 multiply_convert_fusion.2
  74.2 0.0 all-gather.5.cloned.1.call-update
  74.2 11.2 %collective-permute-done.4 = bf16[512,512]{1,0:T(8,128)(2,1)} collective-permute-done((bf16[512,512]{1,0:T(8,128)(2,1)S(1)}, bf16[512,512]{1,0:T(8,128)(2,1)}, u32[]{:S(2)}, u32[]{:S(2)}) %collective-permute-start.4) | collective-permute-done | bytes 524320 | tf_op jit(solution)/shard_map/ppermute | solution.py:13
  85.4 0.0 collective-permute-start.5
  85.4 27.1 %collective-permute-done.5 = bf16[512,512]{1,0:T(8,128)(2,1)} collective-permute-done((bf16[512,512]{1,0:T(8,128)(2,1)}, bf16[512,512]{1,0:T(8,128)(2,1)}, u32[]{:S(2)}, u32[]{:S(2)}) %collective-permute-start.5) | collective-permute-done | bytes 524320 | tf_op jit(solution)/shard_map/ppermute | solution.py:13
  112.5 0.0 collective-permute-start.6
  112.5 13.8 %collective-permute-done.6 = bf16[512,512]{1,0:T(8,128)(2,1)} collective-permute-done((bf16[512,512]{1,0:T(8,128)(2,1)}, bf16[512,512]{1,0:T(8,128)(2,1)}, u32[]{:S(2)}, u32[]{:S(2)}) %collective-permute-start.6) | collective-permute-done | bytes 524320 | tf_op jit(solution)/shard_map/ppermute | solution.py:13
  126.3 1.1 constant_dynamic-update-slice_fusion.15
  127.4 1.1 constant_dynamic-update-slice_fusion.14
  128.4 1.1 constant_dynamic-update-slice_fusion.13
  129.7 0.0 copy-done
  129.7 0.1 constant_dynamic-update-slice_fusion.8
  129.8 1.1 constant_dynamic-update-slice_fusion.7
  130.9 1.1 constant_dynamic-update-slice_fusion.6
  131.9 1.1 constant_dynamic-update-slice_fusion.5
  133.2 0.1 constant_dynamic-update-slice_fusion
  133.3 2.3 constant_dynamic-slice_fusion
  135.6 4.9 %all-to-all-start = ((bf16[4,1024,512]{2,1,0:T(8,128)(2,1)}), bf16[4,1024,512]{2,1,0:T(8,128)(2,1)}, u32[]{:S(2)}, u32[]{:S(2)}) async-start(bf16[4,1024,512]{2,1,0:T(8,128)(2,1)} %bitcast.7), calls=%async_computation | async-start | bytes 8388608 | tf_op jit(solution)/shard_map/all_to_all | solution.py:17
  140.5 0.0 reduce-scatter.2.cloned.1.call-start
  140.6 0.0 all-gather.3.cloned.1.call-done
  140.6 3.1 %fusion = f32[1024]{0:T(1024)S(1)} fusion(bf16[1024,2048]{1,0:T(8,128)(2,1)} %all-gather.3.cloned.1.call-done), kind=kLoop, calls=%fused_computation.2 | loop fusion | flops 6290432 | bytes 4198400 | tf_op jit(solution)/shard_map/reduce_sum | solution.py:20
  143.7 45.0 %all-to-all-done = bf16[4,1024,512]{2,1,0:T(8,128)(2,1)} async-done(((bf16[4,1024,512]{2,1,0:T(8,128)(2,1)}), bf16[4,1024,512]{2,1,0:T(8,128)(2,1)}, u32[]{:S(2)}, u32[]{:S(2)}) %all-to-all-start) | async-done | bytes 4194336 | tf_op jit(solution)/shard_map/all_to_all | solution.py:17
  188.7 6.2 %copy.7 = bf16[1024,4,512]{0,2,1:T(8,128)(2,1)} copy(bf16[1024,4,512]{2,0,1:T(8,128)(2,1)} %bitcast.1) | data formatting | bytes 8388608 | tf_op jit(solution)/shard_map/all_to_all | solution.py:17
  194.9 0.0 all-gather.5.cloned.1.call-done
  194.9 14.7 %convolution_convert_fusion = bf16[1024,2048]{1,0:T(8,128)(2,1)} fusion(bf16[1024,2048]{0,1:T(8,128)(2,1)} %bitcast.5, bf16[2048,1024]{1,0:T(8,128)(2,1)} %all-gather.5.cloned.1.call-done, bf16[1024,2048]{1,0:T(8,128)(2,1)} %all-gather.3.cloned.1.call-done, f32[1024]{0:T(1024)S(1)} %add_rsqrt_fusion), kind=kOutput, calls=%fused_computation.7 | convolution fusion | flops 8601468928 | bytes 16781312 | tf_op jit(solution)/shard_map/dot_general | solution.py:24
  209.6 0.0 reduce-scatter.2.cloned.1.call-update
  209.7 6.6 %copy.8 = bf16[1024,2048]{1,0:T(8,128)(2,1)} copy(bf16[1024,2048]{0,1:T(8,128)(2,1)} %bitcast.6) | data formatting | bytes 8388608
  216.3 34.0 %reduce-scatter.2.cloned.1.call-done = bf16[1024,512]{1,0:T(8,128)(2,1)} async-done(((bf16[1024,2048]{1,0:T(8,128)(2,1)}), bf16[1024,512]{1,0:T(8,128)(2,1)}) %reduce-scatter.2.cloned.1.call-update) | async-done | bytes 1048592 | tf_op jit(solution)/shard_map/reduce_scatter | solution.py:25
  250.4 4.6 %copy.25 = bf16[2048,1024]{1,0:T(8,128)(2,1)} copy(bf16[2048,1024]{1,0:T(8,128)(2,1)} %all-gather.5.cloned.1.call-done) | data formatting | bytes 8388608
  (9 shorter events, 0.3 us)
Async XLA Ops:
  7.2 122.5 %copy-start = (f32[512,512]{1,0:T(8,128)S(1)}, f32[512,512]{1,0:T(8,128)}, u32[]{:S(2)}) copy-start(f32[512,512]{1,0:T(8,128)} %param.7) | copy-start | bytes 3145732
  7.2 133.4 %all-gather.3.cloned.1.call-start = ((), (), s32[]{:S(2)}) async-start(), calls=%async_computation.2 | async-start | bytes 5242880 | tf_op jit(solution)/shard_map/all_gather | solution.py:18
  7.9 187.0 %all-gather.5.cloned.1.call-start = ((), (), s32[]{:S(2)}) async-start(), calls=%async_computation.3 | async-start | bytes 4718592 | tf_op jit(solution)/shard_map/all_gather | solution.py:9
  9.2 18.0 %collective-permute-start = (bf16[512,512]{1,0:T(8,128)(2,1)S(1)}, bf16[512,512]{1,0:T(8,128)(2,1)S(1)}, u32[]{:S(2)}, u32[]{:S(2)}) collective-permute-start(bf16[512,512]{1,0:T(8,128)(2,1)S(1)} %convert_element_type.22), channel_id=1, source_target_pairs={{0,4},{4,8},{8,12},{12,16},{16,20},{20,24},{24,28},{28,0},{1,5},{5... | collective-permute-start | bytes 1572872 | tf_op jit(solution)/shard_map/ppermute | solution.py:13
  27.3 15.8 %collective-permute-start.1 = (bf16[512,512]{1,0:T(8,128)(2,1)S(1)}, bf16[512,512]{1,0:T(8,128)(2,1)S(1)}, u32[]{:S(2)}, u32[]{:S(2)}) collective-permute-start(bf16[512,512]{1,0:T(8,128)(2,1)S(1)} %collective-permute-done), channel_id=1, source_target_pairs={{0,4},{4,8},{8,12},{12,16},{16,20},{20,24},{24,28},{28,0},{1,5},{5... | collective-permute-start | bytes 1572872 | tf_op jit(solution)/shard_map/ppermute | solution.py:13
  43.0 14.9 %collective-permute-start.2 = (bf16[512,512]{1,0:T(8,128)(2,1)S(1)}, bf16[512,512]{1,0:T(8,128)(2,1)S(1)}, u32[]{:S(2)}, u32[]{:S(2)}) collective-permute-start(bf16[512,512]{1,0:T(8,128)(2,1)S(1)} %collective-permute-done.1), channel_id=1, source_target_pairs={{0,4},{4,8},{8,12},{12,16},{16,20},{20,24},{24,28},{28,0},{1,5},{5... | collective-permute-start | bytes 1572872 | tf_op jit(solution)/shard_map/ppermute | solution.py:13
  58.0 14.1 %collective-permute-start.3 = (bf16[512,512]{1,0:T(8,128)(2,1)S(1)}, bf16[512,512]{1,0:T(8,128)(2,1)S(1)}, u32[]{:S(2)}, u32[]{:S(2)}) collective-permute-start(bf16[512,512]{1,0:T(8,128)(2,1)S(1)} %collective-permute-done.2), channel_id=1, source_target_pairs={{0,4},{4,8},{8,12},{12,16},{16,20},{20,24},{24,28},{28,0},{1,5},{5... | collective-permute-start | bytes 1572872 | tf_op jit(solution)/shard_map/ppermute | solution.py:13
  72.0 13.3 %collective-permute-start.4 = (bf16[512,512]{1,0:T(8,128)(2,1)S(1)}, bf16[512,512]{1,0:T(8,128)(2,1)}, u32[]{:S(2)}, u32[]{:S(2)}) collective-permute-start(bf16[512,512]{1,0:T(8,128)(2,1)S(1)} %collective-permute-done.3), channel_id=1, source_target_pairs={{0,4},{4,8},{8,12},{12,16},{16,20},{20,24},{24,28},{28,0},{1,5},{5... | collective-permute-start | bytes 1572872 | tf_op jit(solution)/shard_map/ppermute | solution.py:13
  85.4 27.1 %collective-permute-start.5 = (bf16[512,512]{1,0:T(8,128)(2,1)}, bf16[512,512]{1,0:T(8,128)(2,1)}, u32[]{:S(2)}, u32[]{:S(2)}) collective-permute-start(bf16[512,512]{1,0:T(8,128)(2,1)} %collective-permute-done.4), channel_id=1, source_target_pairs={{0,4},{4,8},{8,12},{12,16},{16,20},{20,24},{24,28},{28,0},{1,5},{5... | collective-permute-start | bytes 1572872 | tf_op jit(solution)/shard_map/ppermute | solution.py:13
  112.5 13.8 %collective-permute-start.6 = (bf16[512,512]{1,0:T(8,128)(2,1)}, bf16[512,512]{1,0:T(8,128)(2,1)}, u32[]{:S(2)}, u32[]{:S(2)}) collective-permute-start(bf16[512,512]{1,0:T(8,128)(2,1)} %collective-permute-done.5), channel_id=1, source_target_pairs={{0,4},{4,8},{8,12},{12,16},{16,20},{20,24},{24,28},{28,0},{1,5},{5... | collective-permute-start | bytes 1572872 | tf_op jit(solution)/shard_map/ppermute | solution.py:13
  135.6 53.1 %all-to-all-start = ((bf16[4,1024,512]{2,1,0:T(8,128)(2,1)}), bf16[4,1024,512]{2,1,0:T(8,128)(2,1)}, u32[]{:S(2)}, u32[]{:S(2)}) async-start(bf16[4,1024,512]{2,1,0:T(8,128)(2,1)} %bitcast.7), calls=%async_computation | async-start | bytes 8388608 | tf_op jit(solution)/shard_map/all_to_all | solution.py:17
  140.5 109.8 %reduce-scatter.2.cloned.1.call-start = ((), (), s32[]{:S(2)}) async-start(), calls=%async_computation.4 | async-start | bytes 5242880 | tf_op jit(solution)/shard_map/reduce_scatter | solution.py:25
Sparse Core Ops, SparseCore 0:
  9.5 37.1 all-gather.2
  74.3 86.3 all-gather.4
  209.8 40.5 reduce-scatter.1
